TPU v7x, 32 devices: a whole 2x2x4 slice. The times are simulated.
32 devices in a mesh: grp: 2 (over y), row: 4 (over z), col: 4 (over x, core).
Axes of the slice: x: 2, y: 2, z: 4, core: 2. Of those that a mesh axis runs over, the one named last changes fastest.
Arguments:
- tokens: bfloat16 [5120, 2048], P(('grp', 'row')), parts along dimension 0, may hold values from -6 to 6
- w_four: bfloat16 [2048, 1024], P(None, 'col'), may hold values from -0.125 to 0.125
- w_gate: bfloat16 [2048, 2048], P(None, 'col'), may hold values from -0.125 to 0.125
- w_back: bfloat16 [1024, 2048], P(None, 'col'), may hold values from -0.1875 to 0.1875
Outputs:
- mixed: bfloat16 [5120, 2048], P(('grp', 'row'), 'col'), parts along dimension 0
There are 2 independent parts, one for each index of `grp`. A program takes and returns all parts, laid end to end along the dimension named above; an argument that names none is the same for every part. Nothing has to cross between parts.
All inputs are finite; a program needn't handle non-finite values.
Results may differ from a plain program's by a relative error of at most 0.0085.
Values may be sent and summed in bfloat16 or wider, within the bound.
A program may use at most 64 MiB of HBM per device.

v0:
```python
import math
import jax
import jax.numpy as jnp
from jax import lax
from jax.sharding import PartitionSpec as P

GROUP_DIM = 128


def tables(count_len):
    steps = lax.iota(jnp.int32, count_len)
    product = steps[:, None] * steps[None, :] % count_len
    angles = product.astype(jnp.float32) * (2.0 * math.pi / count_len)
    return (jnp.cos(angles), jnp.sin(angles))


def channel_mix(values, matrix):
    height = values.shape[0]
    shaped = values.reshape(height, -1, GROUP_DIM)
    mixed_ch = jnp.einsum("ngc,cj->ngj", shaped, matrix, precision=lax.Precision.HIGHEST)
    return mixed_ch.reshape(height, -1)


def across_rows(values, matrix):
    return jnp.einsum("kr,rmc->kmc", matrix, values, precision=lax.Precision.HIGHEST)


def long_transform(col_re, col_im):
    length = col_re.shape[0]
    first_len = 8
    second_len = length // first_len
    shaped_re = col_re.reshape(first_len, second_len, -1)
    shaped_im = col_im.reshape(first_len, second_len, -1)
    cos_first, sin_first = tables(first_len)
    cos_second, sin_second = tables(second_len)
    section_re = across_rows(shaped_re, cos_first) + across_rows(shaped_im, sin_first)
    section_im = across_rows(shaped_im, cos_first) - across_rows(shaped_re, sin_first)
    outer = lax.iota(jnp.int32, first_len)[:, None]
    inner = lax.iota(jnp.int32, second_len)[None, :]
    angle = (outer * inner % length).astype(jnp.float32) * (2.0 * math.pi / length)
    turn_cos = jnp.cos(angle)[:, :, None]
    turn_sin = jnp.sin(angle)[:, :, None]
    bent_re = section_re * turn_cos + section_im * turn_sin
    bent_im = section_im * turn_cos - section_re * turn_sin
    final_re = jnp.einsum("qb,kbc->qkc", cos_second, bent_re, precision=lax.Precision.HIGHEST)
    final_re = final_re + jnp.einsum(
        "qb,kbc->qkc", sin_second, bent_im, precision=lax.Precision.HIGHEST
    )
    final_re = final_re.reshape(length, -1)
    final_im = jnp.einsum("qb,kbc->qkc", cos_second, bent_im, precision=lax.Precision.HIGHEST)
    final_im = final_im - jnp.einsum(
        "qb,kbc->qkc", sin_second, bent_re, precision=lax.Precision.HIGHEST
    )
    return (final_re, final_im.reshape(length, -1))


def on_device(tokens, w_four, w_gate, w_back):
    length = tokens.shape[0]
    row_count = lax.axis_size("row")
    row_index = lax.axis_index("row")
    piece_rows = length // row_count
    total_len = length * row_count
    feats = jnp.dot(tokens, w_four, preferred_element_type=jnp.float32).astype(jnp.bfloat16)
    lifted = feats.astype(jnp.float32)
    cos_group, sin_group = tables(GROUP_DIM)
    cos_rows, sin_rows = tables(row_count)
    residue = lax.iota(jnp.int32, row_count)[:, None]
    within = row_index * piece_rows + lax.iota(jnp.int32, piece_rows)[None, :]
    twist = (residue * within % total_len).astype(jnp.float32) * (2.0 * math.pi / total_len)
    twist_cos = jnp.cos(twist)[:, :, None]
    twist_sin = jnp.sin(twist)[:, :, None]
    line_re = lax.all_to_all(
        lifted[None].astype(jnp.bfloat16), "row", split_axis=1, concat_axis=0, tiled=True
    ).astype(jnp.float32)
    freq_re = across_rows(line_re, cos_rows)
    freq_im = -across_rows(line_re, sin_rows)
    turned_re = freq_re * twist_cos + freq_im * twist_sin
    turned_im = freq_im * twist_cos - freq_re * twist_sin
    col_re, col_im = (
        lax.all_to_all(turned_re, "row", split_axis=0, concat_axis=1, tiled=True),
        lax.all_to_all(turned_im, "row", split_axis=0, concat_axis=1, tiled=True),
    )
    col_re = col_re.reshape(length, -1)
    col_im = col_im.reshape(length, -1)
    whole_re, whole_im = long_transform(col_re, col_im)
    result = channel_mix(whole_re, cos_group) + channel_mix(whole_im, sin_group)
    scaled = (result * (1.0 / math.sqrt(total_len * GROUP_DIM))).astype(jnp.bfloat16)
    ordered = lax.all_to_all(scaled[:, None], "row", split_axis=0, concat_axis=1, tiled=True)
    ordered = ordered.reshape(length, -1)
    proj = jnp.dot(
        lax.all_gather(ordered, "col", axis=1, tiled=True),
        w_back,
        preferred_element_type=jnp.float32,
    )
    gate = jax.nn.sigmoid(jnp.dot(tokens, w_gate, preferred_element_type=jnp.float32))
    return (gate * proj).astype(jnp.bfloat16)


def solution(mesh):
    return jax.shard_map(
        on_device,
        mesh=mesh,
        in_specs=(P(("grp", "row"), None), P(None, "col"), P(None, "col"), P(None, "col")),
        out_specs=P(("grp", "row"), "col"),
        check_vma=False,
    )
```

profile of v0, /device:TPU:0, one launch (start us, length us, event | category | flops | bytes accessed | tf_op | source)
XLA Modules:
  0.0 142.1 jit_solution(10061951131345919692)
XLA Ops:
  6.5 1.7 %copy-done = bf16[640,2048]{1,0:T(8,128)(2,1)S(1)} copy-done((bf16[640,2048]{1,0:T(8,128)(2,1)S(1)}, bf16[640,2048]{1,0:T(8,128)(2,1)}, u32[]{:S(2)}) %copy-start) | copy-done | bytes 2621464
  8.3 2.1 %fusion.6 = bf16[1,640,256]{2,1,0:T(8,128)(2,1)S(1)} fusion(bf16[640,2048]{1,0:T(8,128)(2,1)S(1)} %copy-done, bf16[2048,256]{1,0:T(8,128)(2,1)} %param.5), kind=kOutput, calls=%fused_computation.15 | convolution fusion | flops 671252480 | bytes 3997696 | tf_op jit(solution)/shard_map/dot_general | solution.py:63
  11.4 3.3 %reduce = bf16[640,256]{1,0:T(8,128)(2,1)} reduce(bf16[640,1,256]{2,1,0:T(2,128)(2,1)S(1)} %bitcast.61, bf16[]{:T(256)} %broadcast.193), dimensions={1}, to_apply=%bitcast.56.reduce_sub_computation | reduce | bytes 655362
  14.7 1.8 %reshape.136 = bf16[4,2,20480]{2,1,0:T(2,128)(2,1)} reshape(bf16[640,256]{1,0:T(8,128)(2,1)} %reduce) | data formatting | bytes 655360
  16.5 6.3 %all-to-all-start = ((bf16[4,2,20480]{2,1,0:T(2,128)(2,1)}), bf16[4,2,20480]{2,1,0:T(2,128)(2,1)}, u32[]{:S(2)}, u32[]{:S(2)}) async-start(bf16[4,2,20480]{2,1,0:T(2,128)(2,1)} %reshape.136), calls=%async_computation | async-start | bytes 655360 | tf_op jit(solution)/shard_map/all_to_all | solution.py:72
  23.2 10.1 %all-to-all-done = bf16[4,2,20480]{2,1,0:T(2,128)(2,1)} async-done(((bf16[4,2,20480]{2,1,0:T(2,128)(2,1)}), bf16[4,2,20480]{2,1,0:T(2,128)(2,1)}, u32[]{:S(2)}, u32[]{:S(2)}) %all-to-all-start) | async-done | bytes 327712 | tf_op jit(solution)/shard_map/all_to_all | solution.py:72
  33.3 1.2 reshape.137
  35.3 2.0 %multiply_add_fusion.1 = (f32[4,160,256]{2,0,1:T(4,128)S(1)}, f32[4,160,256]{2,0,1:T(4,128)}) fusion(f32[4,160,256]{2,0,1:T(4,128)S(1)} %fusion.23, f32[4,160]{0,1:T(8,128)S(1)} %copy.69, f32[4,160]{0,1:T(8,128)S(1)} %copy.67, bf16[4,160,256]{2,1,0:T(8,128)(2,1)S(1)} %bitcast.65), kind=kOutput, calls=%fused_computation.22 | convolution fusion | flops 9011424 | bytes 2298880 | tf_op jit(solution)/shard_map/kr,rmc->kmc/dot_general | solution.py:25
  38.3 3.5 %all-to-all-start.1 = ((f32[4,160,256]{2,1,0:T(8,128)}), f32[4,160,256]{2,1,0:T(8,128)S(1)}, u32[]{:S(2)}, u32[]{:S(2)}) async-start(f32[4,160,256]{2,1,0:T(8,128)} %copy.70), calls=%async_computation.1 | async-start | bytes 1310720 | tf_op jit(solution)/shard_map/all_to_all | solution.py:80
  41.8 2.1 %copy.72 = f32[4,160,256]{2,1,0:T(8,128)} copy(f32[4,160,256]{2,0,1:T(4,128)} %get-tuple-element.6) | data formatting | bytes 1310720 | tf_op jit(solution)/shard_map/sub | solution.py:78
  43.9 13.6 %all-to-all-done.1 = f32[4,160,256]{2,1,0:T(8,128)S(1)} async-done(((f32[4,160,256]{2,1,0:T(8,128)}), f32[4,160,256]{2,1,0:T(8,128)S(1)}, u32[]{:S(2)}, u32[]{:S(2)}) %all-to-all-start.1) | async-done | bytes 655392 | tf_op jit(solution)/shard_map/all_to_all | solution.py:80
  58.3 3.5 %all-to-all-start.2 = ((f32[4,160,256]{2,1,0:T(8,128)}), f32[4,160,256]{2,1,0:T(8,128)S(1)}, u32[]{:S(2)}, u32[]{:S(2)}) async-start(f32[4,160,256]{2,1,0:T(8,128)} %copy.72), calls=%async_computation.2 | async-start | bytes 1310720 | tf_op jit(solution)/shard_map/all_to_all | solution.py:81
  62.3 2.9 %fusion.20 = f32[8,80,256]{2,0,1:T(8,128)} fusion(f32[8,80,256]{2,1,0:T(8,128)} %bitcast.59), kind=kOutput, calls=%fused_computation.33 | convolution fusion | flops 15729536 | bytes 1310720 | tf_op jit(solution)/shard_map/kr,rmc->kmc/dot_general | solution.py:25
  65.2 13.1 %all-to-all-done.2 = f32[4,160,256]{2,1,0:T(8,128)S(1)} async-done(((f32[4,160,256]{2,1,0:T(8,128)}), f32[4,160,256]{2,1,0:T(8,128)S(1)}, u32[]{:S(2)}, u32[]{:S(2)}) %all-to-all-start.2) | async-done | bytes 655392 | tf_op jit(solution)/shard_map/all_to_all | solution.py:81
  83.6 1.8 %convolution_subtract_fusion = f32[80,8,256]{2,0,1:T(8,128)} fusion(f32[80,8,256]{2,0,1:T(8,128)S(1)} %fusion.10, f32[8,80,256]{2,0,1:T(8,128)S(1)} %get-tuple-element.8), kind=kOutput, calls=%fused_computation.7 | convolution fusion | flops 157507840 | bytes 1966080 | tf_op jit(solution)/shard_map/qb,kbc->qkc/dot_general | solution.py:51
  88.0 2.1 %fusion.8 = f32[640,2,128]{0,2,1:T(8,128)S(1)} fusion(f32[640,2,128]{2,1,0:T(2,128)} %reshape_reshape.14), kind=kOutput, calls=%fused_computation.17 | convolution fusion | flops 251887616 | bytes 1310720 | tf_op jit(solution)/shard_map/ngc,cj->ngj/dot_general | solution.py:20
  91.4 2.3 %reshape_reshape.15 = f32[640,2,128]{2,1,0:T(2,128)} reshape(f32[80,8,256]{2,1,0:T(8,128)} %copy.84) | data formatting | bytes 1310720 | tf_op jit(solution)/shard_map/reshape;reshape | solution.py:19
  93.6 2.8 %fusion.5 = bf16[640,2,128]{0,2,1:T(8,128)(2,1)} fusion(f32[640,2,128]{0,2,1:T(8,128)S(1)} %fusion.8, f32[640,2,128]{2,1,0:T(2,128)} %reshape_reshape.15), kind=kOutput, calls=%fused_computation.13 | convolution fusion | flops 252379136 | bytes 1638400 | tf_op jit(solution)/shard_map/ngc,cj->ngj/dot_general | solution.py:20
  96.4 1.8 %reduce.1 = bf16[640,256]{0,1:T(8,128)(2,1)S(1)} reduce(bf16[640,1,256]{0,2,1:T(8,128)(2,1)} %bitcast.66, bf16[]{:T(256)} %broadcast.193), dimensions={1}, to_apply=%copy.86.reduce_sub_computation | reduce | bytes 655362 | tf_op jit(solution)/shard_map/convert_element_type | solution.py:87
  98.6 12.9 %all_to_all.45 = bf16[4,2,20480]{2,1,0:T(2,128)(2,1)} all-to-all(bf16[4,2,20480]{2,1,0:T(2,128)(2,1)S(1)} %reshape.138), channel_id=1, replica_groups=mesh['grp'=2,'row'=4,'col'=4] {'row'}, dimensions={0} | all-to-all | bytes 655360 | tf_op jit(solution)/shard_map/all_to_all | solution.py:88
  111.6 1.2 reshape.139
  114.0 4.3 %fusion.2 = f32[640,512]{1,0:T(8,128)} fusion(bf16[640,2048]{1,0:T(8,128)(2,1)S(1)} %copy-done, bf16[2048,512]{1,0:T(8,128)(2,1)} %param.6), kind=kOutput, calls=%fused_computation.4 | convolution fusion | flops 1343160320 | bytes 6029312 | tf_op jit(solution)/shard_map/dot_general | solution.py:95
  118.3 13.2 %all-gather.2.cloned.1.call-done = bf16[640,1024]{1,0:T(8,128)(2,1)} async-done(((bf16[640,256]{1,0:T(8,128)(2,1)}), bf16[640,1024]{1,0:T(8,128)(2,1)}) %all-gather.2.cloned.1.call-update) | async-done | bytes 1310736 | tf_op jit(solution)/shard_map/all_gather | solution.py:91
  131.5 3.7 %fusion.3 = bf16[640,512]{1,0:T(8,128)(2,1)} fusion(f32[640,512]{1,0:T(8,128)} %fusion.2, bf16[640,1024]{1,0:T(8,128)(2,1)} %all-gather.2.cloned.1.call-done, bf16[1024,512]{1,0:T(8,128)(2,1)} %param.7), kind=kOutput, calls=%fused_computation.5 | convolution fusion | flops 671744000 | bytes 4325376 | tf_op jit(solution)/shard_map/dot_general | solution.py:90
  (38 shorter events, 15.1 us)
Async XLA Ops:
  6.5 1.7 %copy-start = (bf16[640,2048]{1,0:T(8,128)(2,1)S(1)}, bf16[640,2048]{1,0:T(8,128)(2,1)}, u32[]{:S(2)}) copy-start(bf16[640,2048]{1,0:T(8,128)(2,1)} %param.4) | copy-start | bytes 7864324
  16.5 16.8 %all-to-all-start = ((bf16[4,2,20480]{2,1,0:T(2,128)(2,1)}), bf16[4,2,20480]{2,1,0:T(2,128)(2,1)}, u32[]{:S(2)}, u32[]{:S(2)}) async-start(bf16[4,2,20480]{2,1,0:T(2,128)(2,1)} %reshape.136), calls=%async_computation | async-start | bytes 655360 | tf_op jit(solution)/shard_map/all_to_all | solution.py:72
  38.3 19.1 %all-to-all-start.1 = ((f32[4,160,256]{2,1,0:T(8,128)}), f32[4,160,256]{2,1,0:T(8,128)S(1)}, u32[]{:S(2)}, u32[]{:S(2)}) async-start(f32[4,160,256]{2,1,0:T(8,128)} %copy.70), calls=%async_computation.1 | async-start | bytes 1310720 | tf_op jit(solution)/shard_map/all_to_all | solution.py:80
  57.4 0.8 copy-start.1
  58.3 20.0 %all-to-all-start.2 = ((f32[4,160,256]{2,1,0:T(8,128)}), f32[4,160,256]{2,1,0:T(8,128)S(1)}, u32[]{:S(2)}, u32[]{:S(2)}) async-start(f32[4,160,256]{2,1,0:T(8,128)} %copy.72), calls=%async_computation.2 | async-start | bytes 1310720 | tf_op jit(solution)/shard_map/all_to_all | solution.py:81
  61.8 69.8 %all-gather.2.cloned.1.call-start = ((), (), s32[]{:S(2)}) async-start(), calls=%async_computation.4 | async-start | bytes 1638400 | tf_op jit(solution)/shard_map/all_gather | solution.py:91
  78.3 1.1 copy-start.2
  79.4 1.1 copy-start.3
  88.0 2.1 %copy-start.4 = (f32[80,8,256]{2,0,1:T(8,128)S(1)}, f32[80,8,256]{2,0,1:T(8,128)}, u32[]{:S(2)}) copy-start(f32[80,8,256]{2,0,1:T(8,128)} %convolution_subtract_fusion) | copy-start | bytes 1966084
Sparse Core Ops, SparseCore 0:
  114.1 17.4 all-gather.1
where the time goes:
time: 143 us; the launch traced here: 142 us
  waiting for transfers between devices  50 us (35%)
  matrix products  28.6 us (20%)
  local copies, waits for them, and re-layouts  18.2 us (13%)
  between operations  13.6 us (10%)
  starting transfers between devices  13.5 us (9%)
  blocking collectives  12.9 us (9%)
  other arithmetic  5.24 us (4%)
    all_to_all x1, waiting for transfers between devices, on_device(): lax.all_to_all(turned_re, 'row', split_axis=0, concat_axis=1, tiled=True)  13.6 us
    all_gather x1, waiting for transfers between devices, on_device(): lax.all_gather(ordered, 'col', axis=1, tiled=True)  13.2 us
    all_to_all x1, waiting for transfers between devices, on_device(): lax.all_to_all(turned_im, 'row', split_axis=0, concat_axis=1, tiled=True)  13.1 us
    all_to_all x1, blocking collectives, on_device(): lax.all_to_all(scaled[:, None], 'row', split_axis=0, concat_axis=1, tiled...  12.9 us
    all_to_all x1, waiting for transfers between devices, on_device(): lax.all_to_all(lifted[None].astype(jnp.bfloat16), 'row', split_axis=1, co...  10.1 us
    dot_general x6, matrix products, across_rows(): jnp.einsum('kr,rmc->kmc', matrix, values, precision=lax.Precision.HIGHEST)  8.85 us
    unnamed x18, local copies, waits for them, and re-layouts  8.15 us
    all_to_all x1, starting transfers between devices, on_device(): lax.all_to_all(lifted[None].astype(jnp.bfloat16), 'row', split_axis=1, co...  6.35 us
  transfers between devices with their start and end apart: 4, of which 4 were waited for; matrix products, arithmetic and copies ran while one was open for 7% of the time, Pallas kernels for 0%

commit v1 on v0

--- a/solution.py
+++ b/solution.py
@@ -69,8 +69,14 @@
     twist = (residue * within % total_len).astype(jnp.float32) * (2.0 * math.pi / total_len)
     twist_cos = jnp.cos(twist)[:, :, None]
     twist_sin = jnp.sin(twist)[:, :, None]
-    line_re = lax.all_to_all(
-        lifted[None].astype(jnp.bfloat16), "row", split_axis=1, concat_axis=0, tiled=True
+    line_re = jnp.concatenate(
+        lax.all_to_all(
+            jnp.stack(jnp.split(lifted[None].astype(jnp.bfloat16), lax.axis_size("row"), axis=1)),
+            "row",
+            0,
+            0,
+        ),
+        axis=0,
     ).astype(jnp.float32)
     freq_re = across_rows(line_re, cos_rows)
     freq_im = -across_rows(line_re, sin_rows)

time: 143 us -> 137 us (0.958)
  local copies, waits for them, and re-layouts: 18.2 us -> 14.4 us
  other arithmetic: 5.24 us -> 2.7 us
    unnamed x18 -> x14, local copies, waits for them, and re-layouts: 8.15 us -> 4.29 us
    unnamed x1 -> x0, other arithmetic: 3.31 us -> none
where the time goes in v1:
time: 137 us; the launch traced here: 136 us
  waiting for transfers between devices  49.9 us (36%)
  matrix products  28.6 us (21%)
  local copies, waits for them, and re-layouts  14.4 us (11%)
  between operations  13.8 us (10%)
  starting transfers between devices  13.5 us (10%)
  blocking collectives  12.9 us (9%)
  other arithmetic  2.7 us (2%)
    all_to_all x1, waiting for transfers between devices, on_device(): lax.all_to_all(turned_re, 'row', split_axis=0, concat_axis=1, tiled=True)  13.6 us
    all_gather x1, waiting for transfers between devices, on_device(): lax.all_gather(ordered, 'col', axis=1, tiled=True)  13.2 us
    all_to_all x1, waiting for transfers between devices, on_device(): lax.all_to_all(turned_im, 'row', split_axis=0, concat_axis=1, tiled=True)  13.1 us
    all_to_all x1, blocking collectives, on_device(): lax.all_to_all(scaled[:, None], 'row', split_axis=0, concat_axis=1, tiled...  12.9 us
    all_to_all x1, waiting for transfers between devices, on_device(): lax.all_to_all(jnp.stack(jnp.split(lifted[None].astype(jnp.bfloat16), lax...  10 us
    dot_general x6, matrix products, across_rows(): jnp.einsum('kr,rmc->kmc', matrix, values, precision=lax.Precision.HIGHEST)  8.87 us
    all_to_all x1, starting transfers between devices, on_device(): lax.all_to_all(jnp.stack(jnp.split(lifted[None].astype(jnp.bfloat16), lax...  6.35 us
    dot_general x2, matrix products, channel_mix(): jnp.einsum('ngc,cj->ngj', shaped, matrix, precision=lax.Precision.HIGHEST)  4.93 us
  transfers between devices with their start and end apart: 4, of which 4 were waited for; matrix products, arithmetic and copies ran while one was open for 7% of the time, Pallas kernels for 0%

profile of v1, /device:TPU:0, one launch (start us, length us, event | category | flops | bytes accessed | tf_op | source)
XLA Modules:
  0.0 135.9 jit_solution(8198326035737303416)
XLA Ops:
  6.5 1.7 %copy-done = bf16[640,2048]{1,0:T(8,128)(2,1)S(1)} copy-done((bf16[640,2048]{1,0:T(8,128)(2,1)S(1)}, bf16[640,2048]{1,0:T(8,128)(2,1)}, u32[]{:S(2)}) %copy-start) | copy-done | bytes 2621464
  8.3 2.1 %fusion.6 = bf16[1,640,256]{2,1,0:T(8,128)(2,1)S(1)} fusion(bf16[640,2048]{1,0:T(8,128)(2,1)S(1)} %copy-done, bf16[2048,256]{1,0:T(8,128)(2,1)} %param.5), kind=kOutput, calls=%fused_computation.15 | convolution fusion | flops 671252480 | bytes 3997696 | tf_op jit(solution)/shard_map/dot_general | solution.py:63
  11.1 6.3 %all-to-all-start = ((bf16[4,1,160,256]{3,2,1,0:T(8,128)(2,1)}), bf16[4,1,160,256]{3,2,1,0:T(8,128)(2,1)S(1)}, u32[]{:S(2)}, u32[]{:S(2)}) async-start(bf16[4,1,160,256]{3,2,1,0:T(8,128)(2,1)} %pad_maximum_fusion), calls=%async_computation | async-start | bytes 655360 | tf_op jit(solution)/shard_map/all_to_all | solution.py:73
  17.8 10.0 %all-to-all-done = bf16[4,1,160,256]{3,2,1,0:T(8,128)(2,1)S(1)} async-done(((bf16[4,1,160,256]{3,2,1,0:T(8,128)(2,1)}), bf16[4,1,160,256]{3,2,1,0:T(8,128)(2,1)S(1)}, u32[]{:S(2)}, u32[]{:S(2)}) %all-to-all-start) | async-done | bytes 327712 | tf_op jit(solution)/shard_map/all_to_all | solution.py:73
  28.5 2.0 %multiply_add_fusion.1 = (f32[4,160,256]{2,0,1:T(4,128)S(1)}, f32[4,160,256]{2,0,1:T(4,128)}) fusion(f32[4,160,256]{2,0,1:T(4,128)S(1)} %fusion.23, f32[4,160]{0,1:T(8,128)S(1)} %copy.50, f32[4,160]{0,1:T(8,128)S(1)} %copy.48, bf16[4,160,256]{2,1,0:T(8,128)(2,1)S(1)} %bitcast.66), kind=kOutput, calls=%fused_computation.22 | convolution fusion | flops 9011424 | bytes 2298880 | tf_op jit(solution)/shard_map/kr,rmc->kmc/dot_general | solution.py:25
  31.5 3.5 %all-to-all-start.1 = ((f32[4,160,256]{2,1,0:T(8,128)}), f32[4,160,256]{2,1,0:T(8,128)S(1)}, u32[]{:S(2)}, u32[]{:S(2)}) async-start(f32[4,160,256]{2,1,0:T(8,128)} %copy.51), calls=%async_computation.1 | async-start | bytes 1310720 | tf_op jit(solution)/shard_map/all_to_all | solution.py:86
  35.0 2.1 %copy.53 = f32[4,160,256]{2,1,0:T(8,128)} copy(f32[4,160,256]{2,0,1:T(4,128)} %get-tuple-element.6) | data formatting | bytes 1310720 | tf_op jit(solution)/shard_map/sub | solution.py:84
  37.1 13.6 %all-to-all-done.1 = f32[4,160,256]{2,1,0:T(8,128)S(1)} async-done(((f32[4,160,256]{2,1,0:T(8,128)}), f32[4,160,256]{2,1,0:T(8,128)S(1)}, u32[]{:S(2)}, u32[]{:S(2)}) %all-to-all-start.1) | async-done | bytes 655392 | tf_op jit(solution)/shard_map/all_to_all | solution.py:86
  51.5 3.5 %all-to-all-start.2 = ((f32[4,160,256]{2,1,0:T(8,128)}), f32[4,160,256]{2,1,0:T(8,128)S(1)}, u32[]{:S(2)}, u32[]{:S(2)}) async-start(f32[4,160,256]{2,1,0:T(8,128)} %copy.53), calls=%async_computation.2 | async-start | bytes 1310720 | tf_op jit(solution)/shard_map/all_to_all | solution.py:87
  55.5 3.0 %fusion.20 = f32[8,80,256]{2,0,1:T(8,128)} fusion(f32[8,80,256]{2,1,0:T(8,128)} %bitcast.63), kind=kOutput, calls=%fused_computation.33 | convolution fusion | flops 15729536 | bytes 1310720 | tf_op jit(solution)/shard_map/kr,rmc->kmc/dot_general | solution.py:25
  58.5 13.1 %all-to-all-done.2 = f32[4,160,256]{2,1,0:T(8,128)S(1)} async-done(((f32[4,160,256]{2,1,0:T(8,128)}), f32[4,160,256]{2,1,0:T(8,128)S(1)}, u32[]{:S(2)}, u32[]{:S(2)}) %all-to-all-start.2) | async-done | bytes 655392 | tf_op jit(solution)/shard_map/all_to_all | solution.py:87
  73.7 1.2 multiply_subtract_fusion
  76.9 1.8 %convolution_subtract_fusion = f32[80,8,256]{2,0,1:T(8,128)} fusion(f32[80,8,256]{2,0,1:T(8,128)S(1)} %fusion.10, f32[8,80,256]{2,0,1:T(8,128)S(1)} %get-tuple-element.8), kind=kOutput, calls=%fused_computation.7 | convolution fusion | flops 157507840 | bytes 1966080 | tf_op jit(solution)/shard_map/qb,kbc->qkc/dot_general | solution.py:51
  80.1 1.2 reshape_reshape.14
  81.2 2.1 %fusion.8 = f32[640,2,128]{0,2,1:T(8,128)S(1)} fusion(f32[640,2,128]{2,1,0:T(2,128)} %reshape_reshape.14), kind=kOutput, calls=%fused_computation.17 | convolution fusion | flops 251887616 | bytes 1310720 | tf_op jit(solution)/shard_map/ngc,cj->ngj/dot_general | solution.py:20
  83.4 1.2 copy.65
  84.6 2.3 %reshape_reshape.15 = f32[640,2,128]{2,1,0:T(2,128)} reshape(f32[80,8,256]{2,1,0:T(8,128)} %copy.65) | data formatting | bytes 1310720 | tf_op jit(solution)/shard_map/reshape;reshape | solution.py:19
  86.9 2.8 %fusion.5 = bf16[640,2,128]{0,2,1:T(8,128)(2,1)} fusion(f32[640,2,128]{0,2,1:T(8,128)S(1)} %fusion.8, f32[640,2,128]{2,1,0:T(2,128)} %reshape_reshape.15), kind=kOutput, calls=%fused_computation.13 | convolution fusion | flops 252379136 | bytes 1638400 | tf_op jit(solution)/shard_map/ngc,cj->ngj/dot_general | solution.py:20
  90.2 1.8 %reduce = bf16[640,256]{0,1:T(8,128)(2,1)S(1)} reduce(bf16[640,1,256]{0,2,1:T(8,128)(2,1)} %bitcast.68, bf16[]{:T(256)} %broadcast.193), dimensions={1}, to_apply=%copy.67.reduce_sub_computation | reduce | bytes 655362 | tf_op jit(solution)/shard_map/convert_element_type | solution.py:93
  92.5 12.9 %all_to_all.38 = bf16[4,2,20480]{2,1,0:T(2,128)(2,1)} all-to-all(bf16[4,2,20480]{2,1,0:T(2,128)(2,1)S(1)} %reshape.137), channel_id=1, replica_groups=mesh['grp'=2,'row'=4,'col'=4] {'row'}, dimensions={0} | all-to-all | bytes 655360 | tf_op jit(solution)/shard_map/all_to_all | solution.py:94
  105.4 1.2 reshape.138
  107.8 4.4 %fusion.2 = f32[640,512]{1,0:T(8,128)} fusion(bf16[640,2048]{1,0:T(8,128)(2,1)S(1)} %copy-done, bf16[2048,512]{1,0:T(8,128)(2,1)} %param.6), kind=kOutput, calls=%fused_computation.4 | convolution fusion | flops 1343160320 | bytes 6029312 | tf_op jit(solution)/shard_map/dot_general | solution.py:101
  112.1 13.2 %all-gather.2.cloned.1.call-done = bf16[640,1024]{1,0:T(8,128)(2,1)} async-done(((bf16[640,256]{1,0:T(8,128)(2,1)}), bf16[640,1024]{1,0:T(8,128)(2,1)}) %all-gather.2.cloned.1.call-update) | async-done | bytes 1310736 | tf_op jit(solution)/shard_map/all_gather | solution.py:97
  125.3 3.7 %fusion.3 = bf16[640,512]{1,0:T(8,128)(2,1)} fusion(f32[640,512]{1,0:T(8,128)} %fusion.2, bf16[640,1024]{1,0:T(8,128)(2,1)} %all-gather.2.cloned.1.call-done, bf16[1024,512]{1,0:T(8,128)(2,1)} %param.7), kind=kOutput, calls=%fused_computation.5 | convolution fusion | flops 671744000 | bytes 4325376 | tf_op jit(solution)/shard_map/dot_general | solution.py:96
  (35 shorter events, 11.5 us)
Async XLA Ops:
  6.5 1.7 %copy-start = (bf16[640,2048]{1,0:T(8,128)(2,1)S(1)}, bf16[640,2048]{1,0:T(8,128)(2,1)}, u32[]{:S(2)}) copy-start(bf16[640,2048]{1,0:T(8,128)(2,1)} %param.4) | copy-start | bytes 7864324
  11.1 16.7 %all-to-all-start = ((bf16[4,1,160,256]{3,2,1,0:T(8,128)(2,1)}), bf16[4,1,160,256]{3,2,1,0:T(8,128)(2,1)S(1)}, u32[]{:S(2)}, u32[]{:S(2)}) async-start(bf16[4,1,160,256]{3,2,1,0:T(8,128)(2,1)} %pad_maximum_fusion), calls=%async_computation | async-start | bytes 655360 | tf_op jit(solution)/shard_map/all_to_all | solution.py:73
  31.5 19.1 %all-to-all-start.1 = ((f32[4,160,256]{2,1,0:T(8,128)}), f32[4,160,256]{2,1,0:T(8,128)S(1)}, u32[]{:S(2)}, u32[]{:S(2)}) async-start(f32[4,160,256]{2,1,0:T(8,128)} %copy.51), calls=%async_computation.1 | async-start | bytes 1310720 | tf_op jit(solution)/shard_map/all_to_all | solution.py:86
  50.7 0.8 copy-start.1
  51.5 20.0 %all-to-all-start.2 = ((f32[4,160,256]{2,1,0:T(8,128)}), f32[4,160,256]{2,1,0:T(8,128)S(1)}, u32[]{:S(2)}, u32[]{:S(2)}) async-start(f32[4,160,256]{2,1,0:T(8,128)} %copy.53), calls=%async_computation.2 | async-start | bytes 1310720 | tf_op jit(solution)/shard_map/all_to_all | solution.py:87
  55.0 70.3 %all-gather.2.cloned.1.call-start = ((), (), s32[]{:S(2)}) async-start(), calls=%async_computation.4 | async-start | bytes 1638400 | tf_op jit(solution)/shard_map/all_gather | solution.py:97
  71.6 1.1 copy-start.2
  72.6 1.1 copy-start.3
  81.2 2.1 %copy-start.4 = (f32[80,8,256]{2,0,1:T(8,128)S(1)}, f32[80,8,256]{2,0,1:T(8,128)}, u32[]{:S(2)}) copy-start(f32[80,8,256]{2,0,1:T(8,128)} %convolution_subtract_fusion) | copy-start | bytes 1966084
Sparse Core Ops, SparseCore 0:
  107.9 17.4 all-gather.1
